TPU v7x, 32 devices: a whole 2x2x4 slice. The times are simulated.
32 devices in a mesh: ep: 8 (over z, x), tp: 4 (over y, core).
Axes of the slice: x: 2, y: 2, z: 4, core: 2. Of those that a mesh axis runs over, the one named last changes fastest.
Arguments:
- tokens: bfloat16 [256, 2048], P('ep'), may hold values from -6 to 6
- state: float32 [256, 16, 128, 128], P('ep', 'tp'), may hold values from -6 to 6
- norm_gain: float32 [2048], replicated, may hold values from 0.1 to 1.9
- w_query: bfloat16 [2048, 2048], P(None, 'tp'), may hold values from -0.125 to 0.125
- w_forget: bfloat16 [2048, 2048], P(None, 'tp'), may hold values from -0.125 to 0.125
- w_input: bfloat16 [2048, 2048], P(None, 'tp'), may hold values from -0.125 to 0.125
- w_outgate: bfloat16 [2048, 2048], P(None, 'tp'), may hold values from -0.125 to 0.125
- forget_floor: float32 [2048], P('tp'), may hold values from 0.05 to 0.95
- head_gain: float32 [128], replicated, may hold values from 0.1 to 1.9
- w_out: bfloat16 [2048, 2048], P('tp'), may hold values from -0.125 to 0.125
- ffn_gain: float32 [2048], replicated, may hold values from 0.1 to 1.9
- routes: int32 [256, 2], P('ep'), may hold values from 0 to 7, all different within a row; in each aligned block of 32 rows (0 to 31, 32 to 63, ...) at most 16 rows name the same one
- route_weights: float32 [256, 2], P('ep'), may hold values from 0.2 to 1
- expert_gate: bfloat16 [8, 2048, 5632], P('ep', None, 'tp'), may hold values from -0.125 to 0.125
- expert_up: bfloat16 [8, 2048, 5632], P('ep', None, 'tp'), may hold values from -0.125 to 0.125
- expert_down: bfloat16 [8, 5632, 2048], P('ep', 'tp'), may hold values from -0.078125 to 0.078125
- dense_gate: bfloat16 [2048, 5632], P(None, 'ep'), may hold values from -0.125 to 0.125
- dense_up: bfloat16 [2048, 5632], P(None, 'ep'), may hold values from -0.125 to 0.125
- dense_down: bfloat16 [5632, 2048], P('ep'), may hold values from -0.078125 to 0.078125
- dense_mix: float32 [2048], replicated, may hold values from -6 to 6
Outputs:
- mixed: bfloat16 [256, 2048], P('ep')
- new_state: float32 [256, 16, 128, 128], P('ep', 'tp')
Inputs may be any that keep to these rules, and one draw needn't show every extreme that they name: `routes`: each row names 2 different experts; the rows of one index of ep name no expert more than 16 times, a bound that some block reaches.
All inputs are finite; a program needn't handle non-finite values.
Results may differ from a plain program's by a relative error of at most 0.014.
Values may be sent and summed in bfloat16 or wider, within the bound.
A program may use at most 128 MiB of HBM per device.

v0:
```python
import jax
import jax.numpy as jnp
from jax import lax
from jax.sharding import PartitionSpec as P

EPS = 1e-06


def rms_norm(value, gain):
    return value * lax.rsqrt(jnp.mean(value * value, axis=-1, keepdims=True) + EPS) * gain


def make_table(local_routes, experts, capacity):
    flat = local_routes.reshape(-1)
    onehot = (flat[:, None] == jnp.arange(experts, dtype=jnp.int32)[None, :]).astype(jnp.int32)
    before = jnp.cumsum(onehot, axis=0) - onehot
    slot = jnp.sum(before * onehot, axis=1)
    where = flat * capacity + slot
    return (where[:, None] == jnp.arange(experts * capacity, dtype=jnp.int32)[None, :]).astype(
        jnp.bfloat16
    )


def local(
    tokens,
    state,
    norm_gain,
    w_query,
    w_forget,
    w_input,
    w_outgate,
    forget_floor,
    head_gain,
    w_out,
    ffn_gain,
    routes,
    route_weights,
    expert_gate,
    expert_up,
    expert_down,
    dense_gate,
    dense_up,
    dense_down,
    dense_mix,
):
    seqs, width = tokens.shape
    local_heads = state.shape[1]
    key_size = state.shape[2]
    value_size = state.shape[3]
    resid_in = tokens.astype(jnp.float32)
    normed = rms_norm(resid_in, norm_gain).astype(jnp.bfloat16)
    zq = jnp.dot(normed, w_query, preferred_element_type=jnp.float32)
    zf = jnp.dot(normed, w_forget, preferred_element_type=jnp.float32)
    zi = jnp.dot(normed, w_input, preferred_element_type=jnp.float32)
    zg = jnp.dot(normed, w_outgate, preferred_element_type=jnp.float32)
    logf = jnp.logaddexp(jax.nn.log_sigmoid(zf), jnp.log(forget_floor) + jax.nn.log_sigmoid(-zf))
    logf = logf.reshape(seqs, local_heads, key_size)
    query = jax.nn.silu(zq).reshape(seqs, local_heads, key_size)
    keep = jnp.exp(logf)
    write = -jnp.expm1(logf)
    values = zi.reshape(seqs, local_heads, value_size)
    new_state = keep[..., None] * state + write[..., None] * values[:, :, None, :]
    read = jnp.einsum("thk,thkv->thv", query, new_state, precision=lax.Precision.HIGHEST)
    read = rms_norm(read, head_gain).reshape(seqs, local_heads * value_size)
    headout = (read * jax.nn.silu(zg)).astype(jnp.bfloat16)
    block_term = jnp.dot(headout, w_out, preferred_element_type=jnp.float32)
    block_term = block_term.astype(jnp.bfloat16).astype(jnp.float32)
    mixout = lax.psum(block_term.astype(jnp.bfloat16), "tp").astype(jnp.float32)
    resid = resid_in + mixout
    ffn_in = rms_norm(resid, ffn_gain).astype(jnp.bfloat16)
    piece = lax.all_gather(ffn_in, "ep", axis=0, tiled=True)
    dgate = jnp.dot(piece, dense_gate, preferred_element_type=jnp.float32)
    dupper = jnp.dot(piece, dense_up, preferred_element_type=jnp.float32)
    dense_hidden = (jax.nn.silu(dgate) * dupper).astype(jnp.bfloat16)
    rows = dense_hidden
    summed = lax.psum_scatter(
        jnp.dot(rows, dense_down, preferred_element_type=jnp.float32).astype(jnp.bfloat16),
        "ep",
        scatter_dimension=0,
        tiled=True,
    )
    dense = summed.astype(jnp.float32)
    experts = lax.axis_size("ep") * expert_gate.shape[0]
    top = routes.shape[1]
    capacity = 2 * seqs * top // experts
    table = make_table(routes, experts, capacity)
    repeated = jnp.repeat(ffn_in, top, axis=0)
    sent = jnp.dot(table.T, repeated, preferred_element_type=jnp.float32).astype(jnp.bfloat16)
    sent = sent.reshape(experts, capacity, width)
    arrived = lax.all_to_all(sent, "ep", split_axis=0, concat_axis=0, tiled=True)
    sources, items, _ = arrived.shape
    rows = arrived.reshape(sources * items, width)
    gate = jnp.dot(rows, expert_gate[0], preferred_element_type=jnp.float32)
    upper = jnp.dot(rows, expert_up[0], preferred_element_type=jnp.float32)
    hidden = (jax.nn.silu(gate) * upper).astype(jnp.bfloat16)
    part = jnp.dot(hidden, expert_down[0], preferred_element_type=jnp.float32)
    part = part.astype(jnp.bfloat16).astype(jnp.float32)
    summed_parts = lax.psum(part.astype(jnp.bfloat16), "tp")
    results = summed_parts.reshape(sources, items, width)
    back = lax.all_to_all(results, "ep", split_axis=0, concat_axis=0, tiled=True)
    picked = jnp.dot(
        table, back.reshape(experts * capacity, width), preferred_element_type=jnp.float32
    )
    weighted = picked * route_weights.reshape(seqs * top)[:, None]
    moe = jnp.sum(weighted.reshape(seqs, top, width), axis=1)
    mixed = (resid + moe + jax.nn.sigmoid(dense_mix) * dense).astype(jnp.bfloat16)
    return (mixed, new_state)


def solution(mesh):
    in_specs = (
        P("ep", None),
        P("ep", "tp", None, None),
        P(),
        P(None, "tp"),
        P(None, "tp"),
        P(None, "tp"),
        P(None, "tp"),
        P("tp"),
        P(),
        P("tp", None),
        P(),
        P("ep", None),
        P("ep", None),
        P("ep", None, "tp"),
        P("ep", None, "tp"),
        P("ep", "tp", None),
        P(None, "ep"),
        P(None, "ep"),
        P("ep", None),
        P(),
    )
    out_specs = (P("ep", None), P("ep", "tp", None, None))
    return jax.shard_map(local, mesh=mesh, in_specs=in_specs, out_specs=out_specs, check_vma=False)
```

profile of v0, /device:TPU:0, one launch (start us, length us, event | category | flops | bytes accessed | tf_op | source)
XLA Modules:
  0.0 235.8 jit_solution(614285579938243527)
XLA Ops:
  7.2 0.0 copy-start
  7.2 0.0 all-reduce.3.cloned.1.call-start
  7.3 1.2 fusion.20
  8.5 2.2 divide_multiply_fusion
  10.7 2.2 fusion.38
  13.0 2.3 fusion.35
  15.3 8.2 %multiply_add_fusion = f32[32,4,128,128]{3,2,1,0:T(8,128)S(1)} fusion(f32[32,4,128,128]{3,2,1,0:T(8,128)} %param.21, f32[32,4,128]{2,1,0:T(4,128)S(1)} %mul.144, f32[32,4,128]{2,1,0:T(4,128)S(1)} %neg.60, f32[32,4,128]{2,1,0:T(4,128)S(1)} %exp.44), kind=kLoop, calls=%fused_computation | loop fusion | flops 6291456 | bytes 16973824 | tf_op jit(solution)/shard_map/add | solution.py:62
  23.5 0.0 copy-start.1
  23.6 7.3 %fusion.50 = f32[32,4,1,128]{3,2,1,0:T(1,128)S(1)} fusion(f32[32,4,128,1]{2,3,1,0:T(1,128)S(1)} %bitcast.52, f32[32,4,128,128]{3,2,1,0:T(8,128)S(1)} %multiply_add_fusion), kind=kOutput, calls=%fused_computation.59 | convolution fusion | flops 25165824 | bytes 8519680 | tf_op jit(solution)/shard_map/thk,thkv->thv/dot_general | solution.py:63
  30.8 0.1 multiply_reduce_fusion.1
  31.0 0.1 multiply_multiply_fusion
  31.1 3.8 %convolution_convert_fusion.2 = bf16[32,2048]{1,0:T(8,128)(2,1)} fusion(bf16[512,2048]{1,0:T(8,128)(2,1)} %param.29, f32[4,8,4,128]{3,2,1,0:T(4,128)S(1)} %bitcast.53, bf16[2048,512]{1,0:T(8,128)(2,1)} %param.26, bf16[32,2048]{1,0:T(8,128)(2,1)S(1)} %copy-done.2, f32[2048]{0:T(1024)S(1)} %copy-done.4, f32[32]{0:T(128)S(1)} %add_rsqrt_fusion.2), kind=kOutput, calls=%fused_computation.13 | convolution fusion | flops 134643712 | bytes 4530304 | tf_op jit(solution)/shard_map/dot_general | solution.py:66
  34.9 0.0 all-reduce.3.cloned.1.call-update
  35.0 0.1 copy.24
  35.0 0.1 reshape.88
  35.1 0.1 fusion.28
  35.2 0.1 reduce_window_sum.11
  35.3 0.2 select_reduce_fusion
  35.5 34.1 %all-reduce.3.cloned.1.call-done = bf16[32,2048]{1,0:T(8,128)(2,1)} async-done(((bf16[32,2048]{1,0:T(8,128)(2,1)}), bf16[32,2048]{1,0:T(8,128)(2,1)}) %all-reduce.3.cloned.1.call-update) | async-done | bytes 131088 | tf_op jit(solution)/shard_map/psum | solution.py:68
  69.6 1.1 multiply_reduce_fusion
  70.7 1.0 multiply_convert_fusion
  71.7 0.1 broadcast_in_dim.2
  71.9 0.8 reshape.89
  72.6 2.1 convolution_convert_fusion.1
  74.8 5.5 %all-to-all-start = ((bf16[8,16,2048]{2,1,0:T(8,128)(2,1)}), bf16[8,16,2048]{2,1,0:T(8,128)(2,1)S(1)}, u32[]{:S(2)}, u32[]{:S(2)}) async-start(bf16[8,16,2048]{2,1,0:T(8,128)(2,1)} %bitcast.3), calls=%async_computation | async-start | bytes 1048576 | tf_op jit(solution)/shard_map/all_to_all | solution.py:90
  80.3 0.0 all-gather.2.cloned.1.call-start
  80.4 0.7 all-gather.2.cloned.1.call-update
  81.1 0.2 all-reduce.5.cloned.1.call-start
  81.3 12.4 %all-to-all-done = bf16[8,16,2048]{2,1,0:T(8,128)(2,1)S(1)} async-done(((bf16[8,16,2048]{2,1,0:T(8,128)(2,1)}), bf16[8,16,2048]{2,1,0:T(8,128)(2,1)S(1)}, u32[]{:S(2)}, u32[]{:S(2)}) %all-to-all-start) | async-done | bytes 524320 | tf_op jit(solution)/shard_map/all_to_all | solution.py:90
  93.7 4.5 %fusion.4 = f32[128,1408]{1,0:T(8,128)} fusion(bf16[128,2048]{1,0:T(8,128)(2,1)S(1)} %bitcast.47, bf16[1,2048,1408]{2,1,0:T(8,128)(2,1)} %param.33), kind=kOutput, calls=%fused_computation.5 | convolution fusion | flops 738197504 | bytes 7012352 | tf_op jit(solution)/shard_map/dot_general | solution.py:93
  98.2 7.3 %fusion.12 = bf16[128,2048]{1,0:T(8,128)(2,1)} fusion(bf16[1,1408,2048]{2,1,0:T(8,128)(2,1)} %param.35, bf16[128,2048]{1,0:T(8,128)(2,1)S(1)} %bitcast.48, bf16[1,2048,1408]{2,1,0:T(8,128)(2,1)} %param.34, f32[128,1408]{1,0:T(8,128)} %fusion.4), kind=kOutput, calls=%fused_computation.11 | convolution fusion | flops 1477738496 | bytes 13303808 | tf_op jit(solution)/shard_map/dot_general | solution.py:96
  105.5 0.0 all-reduce.5.cloned.1.call-update
  105.5 0.0 reduce-scatter.2.cloned.1.call-start
  105.6 19.0 %all-gather.2.cloned.1.call-done = bf16[256,2048]{1,0:T(8,128)(2,1)} async-done(((bf16[32,2048]{1,0:T(8,128)(2,1)}), bf16[256,2048]{1,0:T(8,128)(2,1)}) %all-gather.2.cloned.1.call-update) | async-done | bytes 1048592 | tf_op jit(solution)/shard_map/all_gather | solution.py:71
  124.6 4.0 %fusion.51 = f32[256,704]{0,1:T(8,128)} fusion(bf16[256,2048]{1,0:T(8,128)(2,1)} %all-gather.2.cloned.1.call-done, bf16[2048,704]{0,1:T(8,128)(2,1)} %param.36), kind=kOutput, calls=%fused_computation.60 | convolution fusion | flops 738197504 | bytes 4653056 | tf_op jit(solution)/shard_map/dot_general | solution.py:72
  128.6 6.6 %convolution_convert_fusion = bf16[256,2048]{1,0:T(8,128)(2,1)} fusion(bf16[704,2048]{1,0:T(8,128)(2,1)S(1)} %copy-done, bf16[256,2048]{1,0:T(8,128)(2,1)} %all-gather.2.cloned.1.call-done, bf16[2048,704]{0,1:T(8,128)(2,1)} %param.37, f32[256,704]{0,1:T(8,128)} %fusion.51), kind=kOutput, calls=%fused_computation.7 | convolution fusion | flops 1478000640 | bytes 8585216 | tf_op jit(solution)/shard_map/dot_general | solution.py:77
  135.2 0.0 reduce-scatter.2.cloned.1.call-update
  135.2 23.9 %all-reduce.5.cloned.1.call-done = bf16[8,16,2048]{2,1,0:T(8,128)(2,1)} async-done(((bf16[8,16,2048]{2,1,0:T(8,128)(2,1)}), bf16[8,16,2048]{2,1,0:T(8,128)(2,1)}) %all-reduce.5.cloned.1.call-update) | async-done | bytes 524304 | tf_op jit(solution)/shard_map/psum | solution.py:98
  159.1 5.5 %all-to-all-start.1 = ((bf16[8,16,2048]{2,1,0:T(8,128)(2,1)}), bf16[8,16,2048]{2,1,0:T(8,128)(2,1)S(1)}, u32[]{:S(2)}, u32[]{:S(2)}) async-start(bf16[8,16,2048]{2,1,0:T(8,128)(2,1)} %all-reduce.5.cloned.1.call-done), calls=%async_computation.1 | async-start | bytes 1048576 | tf_op jit(solution)/shard_map/all_to_all | solution.py:100
  164.6 0.8 copy.25
  165.4 0.6 mul.164
  166.0 0.7 add_divide_fusion
  166.7 15.4 %all-to-all-done.1 = bf16[8,16,2048]{2,1,0:T(8,128)(2,1)S(1)} async-done(((bf16[8,16,2048]{2,1,0:T(8,128)(2,1)}), bf16[8,16,2048]{2,1,0:T(8,128)(2,1)S(1)}, u32[]{:S(2)}, u32[]{:S(2)}) %all-to-all-start.1) | async-done | bytes 524320 | tf_op jit(solution)/shard_map/all_to_all | solution.py:100
  182.1 1.8 convolution_multiply_fusion
  183.8 1.4 reshape.94
  185.2 1.3 reduce_sum.49
  186.5 40.9 %reduce-scatter.2.cloned.1.call-done = bf16[32,2048]{1,0:T(8,128)(2,1)} async-done(((bf16[256,2048]{1,0:T(8,128)(2,1)}), bf16[32,2048]{1,0:T(8,128)(2,1)}) %reduce-scatter.2.cloned.1.call-update) | async-done | bytes 131088 | tf_op jit(solution)/shard_map/reduce_scatter | solution.py:76
  227.5 1.8 add_convert_fusion
  (27 shorter events, 0.2 us)
Async XLA Ops:
  7.2 121.4 %copy-start = (bf16[704,2048]{1,0:T(8,128)(2,1)S(1)}, bf16[704,2048]{1,0:T(8,128)(2,1)}, u32[]{:S(2)}) copy-start(bf16[704,2048]{1,0:T(8,128)(2,1)} %param.38) | copy-start | bytes 8650756
  7.2 5.8 %copy-start.2 = (bf16[32,2048]{1,0:T(8,128)(2,1)S(1)}, bf16[32,2048]{1,0:T(8,128)(2,1)}, u32[]{:S(2)}) copy-start(bf16[32,2048]{1,0:T(8,128)(2,1)} %param.20) | copy-start | bytes 393220
  7.2 5.8 %copy-start.4 = (f32[2048]{0:T(1024)S(1)}, f32[2048]{0:T(1024)}, u32[]{:S(2)}) copy-start(f32[2048]{0:T(1024)} %param.22) | copy-start | bytes 24580
  7.2 5.7 %copy-start.7 = (f32[512]{0:T(512)S(1)}, f32[512]{0:T(512)}, u32[]{:S(2)}) copy-start(f32[512]{0:T(512)} %param.27) | copy-start | bytes 6148
  7.2 62.4 %all-reduce.3.cloned.1.call-start = ((), (), s32[]{:S(2)}) async-start(), calls=%async_computation.3 | async-start | bytes 262144 | tf_op jit(solution)/shard_map/psum | solution.py:68
  23.5 7.3 %copy-start.1 = (f32[32,4,128,128]{3,2,1,0:T(8,128)}, f32[32,4,128,128]{3,2,1,0:T(8,128)S(1)}, u32[]{:S(2)}) copy-start(f32[32,4,128,128]{3,2,1,0:T(8,128)S(1)} %multiply_add_fusion) | copy-start | bytes 25165828
  23.6 7.4 %copy-start.9 = (f32[128]{0:T(128)S(1)}, f32[128]{0:T(128)}, u32[]{:S(2)}) copy-start(f32[128]{0:T(128)} %param.28) | copy-start | bytes 1540
  30.8 4.1 %copy-start.8 = (s32[32,2]{0,1:T(2,128)S(1)}, s32[32,2]{0,1:T(2,128)}, u32[]{:S(2)}) copy-start(s32[32,2]{0,1:T(2,128)} %param.31) | copy-start | bytes 772
  30.8 39.9 %copy-start.5 = (f32[2048]{0:T(1024)S(1)}, f32[2048]{0:T(1024)}, u32[]{:S(2)}) copy-start(f32[2048]{0:T(1024)} %param.30) | copy-start | bytes 24580
  35.5 39.3 %copy-start.6 = (s32[64]{0:T(128)}, s32[64]{0:T(128)S(1)}, u32[]{:S(2)}) copy-start(s32[64]{0:T(128)S(1)} %multiply_add_fusion.1) | copy-start | bytes 772
  71.7 3.1 %copy-start.3 = (bf16[32,2048]{1,0:T(8,128)(2,1)}, bf16[32,2048]{1,0:T(8,128)(2,1)S(1)}, u32[]{:S(2)}) copy-start(bf16[32,2048]{1,0:T(8,128)(2,1)S(1)} %multiply_convert_fusion) | copy-start | bytes 393220
  74.8 18.9 %all-to-all-start = ((bf16[8,16,2048]{2,1,0:T(8,128)(2,1)}), bf16[8,16,2048]{2,1,0:T(8,128)(2,1)S(1)}, u32[]{:S(2)}, u32[]{:S(2)}) async-start(bf16[8,16,2048]{2,1,0:T(8,128)(2,1)} %bitcast.3), calls=%async_computation | async-start | bytes 1048576 | tf_op jit(solution)/shard_map/all_to_all | solution.py:90
  80.3 44.3 %all-gather.2.cloned.1.call-start = ((), (), s32[]{:S(2)}) async-start(), calls=%async_computation.5 | async-start | bytes 1179648 | tf_op jit(solution)/shard_map/all_gather | solution.py:71
  81.1 78.1 %all-reduce.5.cloned.1.call-start = ((), (), s32[]{:S(2)}) async-start(), calls=%async_computation.4 | async-start | bytes 1048576 | tf_op jit(solution)/shard_map/psum | solution.py:98
  105.5 121.9 %reduce-scatter.2.cloned.1.call-start = ((), (), s32[]{:S(2)}) async-start(), calls=%async_computation.6 | async-start | bytes 1179648 | tf_op jit(solution)/shard_map/reduce_scatter | solution.py:76
  159.1 23.0 %all-to-all-start.1 = ((bf16[8,16,2048]{2,1,0:T(8,128)(2,1)}), bf16[8,16,2048]{2,1,0:T(8,128)(2,1)S(1)}, u32[]{:S(2)}, u32[]{:S(2)}) async-start(bf16[8,16,2048]{2,1,0:T(8,128)(2,1)} %all-reduce.5.cloned.1.call-done), calls=%async_computation.1 | async-start | bytes 1048576 | tf_op jit(solution)/shard_map/all_to_all | solution.py:100
Sparse Core Ops, SparseCore 0:
  35.1 34.4 all-reduce.2
  83.8 40.7 all-gather.1
  127.0 32.1 all-reduce.4
  162.4 65.0 reduce-scatter.1
where the time goes:
time: 237 us; the launch traced here: 236 us
  waiting for transfers between devices  147 us (62%)
  matrix products  44 us (19%)
  other arithmetic  15.9 us (7%)
  between operations  14 us (6%)
  starting transfers between devices  11.4 us (5%)
  local copies, waits for them, and re-layouts  4.03 us (2%)
    reduce_scatter x1, waiting for transfers between devices, local(): lax.psum_scatter(jnp.dot(rows, dense_down, preferred_element_type=jnp.flo...  40.9 us
    psum x1, waiting for transfers between devices, local(): mixout = lax.psum(block_term.astype(jnp.bfloat16), 'tp').astype(jnp.float32)  34.1 us
    psum x1, waiting for transfers between devices, local(): summed_parts = lax.psum(part.astype(jnp.bfloat16), 'tp')  23.9 us
    all_gather x1, waiting for transfers between devices, local(): piece = lax.all_gather(ffn_in, 'ep', axis=0, tiled=True)  19 us
    all_to_all x1, waiting for transfers between devices, local(): lax.all_to_all(results, 'ep', split_axis=0, concat_axis=0, tiled=True)  15.4 us
    all_to_all x1, waiting for transfers between devices, local(): lax.all_to_all(sent, 'ep', split_axis=0, concat_axis=0, tiled=True)  12.4 us
    add x1, other arithmetic, local(): keep[..., None] * state + write[..., None] * values[:, :, None, :]  8.22 us
    dot_general x1, matrix products, local(): part = jnp.dot(hidden, expert_down[0], preferred_element_type=jnp.float32)  7.29 us
  transfers between devices with their start and end apart: 6, of which 6 were waited for; matrix products, arithmetic and copies ran while one was open for 12% of the time, Pallas kernels for 0%

commit v1 on v0

--- a/solution.py
+++ b/solution.py
@@ -68,7 +68,13 @@
     mixout = lax.psum(block_term.astype(jnp.bfloat16), "tp").astype(jnp.float32)
     resid = resid_in + mixout
     ffn_in = rms_norm(resid, ffn_gain).astype(jnp.bfloat16)
-    piece = lax.all_gather(ffn_in, "ep", axis=0, tiled=True)
+    define_plane = lambda buf, dim_i: jnp.concatenate(
+        lax.all_to_all(
+            jnp.stack([buf] * lax.axis_size("ep")), axis_name="ep", split_axis=0, concat_axis=0
+        ),
+        dim_i,
+    )
+    piece = define_plane(ffn_in, 0)
     dgate = jnp.dot(piece, dense_gate, preferred_element_type=jnp.float32)
     dupper = jnp.dot(piece, dense_up, preferred_element_type=jnp.float32)
     dense_hidden = (jax.nn.silu(dgate) * dupper).astype(jnp.bfloat16)

time: 237 us -> 222 us (0.937)
  waiting for transfers between devices: 147 us -> 114 us
  blocking collectives: 0 us -> 18.7 us
    all_gather x1 -> x0, waiting for transfers between devices: 19 us -> none  [local(): piece = lax.all_gather(ffn_in, 'ep', axis=0, tiled=True)]
    all_to_all x0 -> x1, blocking collectives: none -> 18.7 us  [local(): lax.all_to_all(sent, 'ep', split_axis=0, concat_axis=0, tiled=True)]
    psum x1, waiting for transfers between devices: 23.9 us -> 10.4 us  [local(): summed_parts = lax.psum(part.astype(jnp.bfloat16), 'tp')]
  transfers between devices with their start and end apart: 6 -> 5, of which waited for: 6 -> 5; matrix products, arithmetic and copies ran while one was open for 12% -> 13% of each run, Pallas kernels for 0% -> 0%
where the time goes in v1:
time: 222 us; the launch traced here: 221 us
  waiting for transfers between devices  114 us (51%)
  matrix products  42.2 us (19%)
  blocking collectives  18.7 us (8%)
  other arithmetic  15.9 us (7%)
  between operations  14 us (6%)
  starting transfers between devices  10.1 us (5%)
  local copies, waits for them, and re-layouts  5.99 us (3%)
    reduce_scatter x1, waiting for transfers between devices, local(): lax.psum_scatter(jnp.dot(rows, dense_down, preferred_element_type=jnp.flo...  41.4 us
    psum x1, waiting for transfers between devices, local(): mixout = lax.psum(block_term.astype(jnp.bfloat16), 'tp').astype(jnp.float32)  34.1 us
    all_to_all x1, blocking collectives, local(): lax.all_to_all(sent, 'ep', split_axis=0, concat_axis=0, tiled=True)  18.7 us
    all_to_all x1, waiting for transfers between devices, local(): lax.all_to_all(results, 'ep', split_axis=0, concat_axis=0, tiled=True)  15.3 us
    all_to_all x1, waiting for transfers between devices, local(): lax.all_to_all(jnp.stack([buf] * lax.axis_size('ep')), axis_name='ep', sp...  13 us
    psum x1, waiting for transfers between devices, local(): summed_parts = lax.psum(part.astype(jnp.bfloat16), 'tp')  10.4 us
    add x1, other arithmetic, local(): keep[..., None] * state + write[..., None] * values[:, :, None, :]  8.22 us
    dot_general x1, matrix products, local(): part = jnp.dot(hidden, expert_down[0], preferred_element_type=jnp.float32)  7.26 us
  transfers between devices with their start and end apart: 5, of which 5 were waited for; matrix products, arithmetic and copies ran while one was open for 13% of the time, Pallas kernels for 0%

profile of v1, /device:TPU:0, one launch (start us, length us, event | category | flops | bytes accessed | tf_op | source)
XLA Modules:
  0.0 221.1 jit_solution(12960436218366852924)
XLA Ops:
  7.2 0.0 copy-start
  7.2 0.0 all-reduce.3.cloned.1.call-start
  7.3 1.2 fusion.20
  8.5 2.2 %divide_multiply_fusion = f32[32,512]{1,0:T(8,128)S(1)} fusion(bf16[2048,512]{1,0:T(8,128)(2,1)} %param.23, bf16[32,2048]{1,0:T(8,128)(2,1)} %param.20, f32[2048]{0:T(1024)} %param.22, f32[32]{0:T(128)S(1)} %add_rsqrt_fusion.2), kind=kOutput, calls=%fused_computation.38 | convolution fusion | flops 67436544 | bytes 2302080 | tf_op jit(solution)/shard_map/dot_general | solution.py:52
  10.7 2.2 fusion.38
  13.0 2.3 %fusion.35 = (f32[32,512]{1,0:T(8,128)S(1)}, f32[32,512]{1,0:T(8,128)S(1)}) fusion(f32[512]{0:T(512)S(1)} %log.3, bf16[2048,512]{1,0:T(8,128)(2,1)} %param.24, bf16[32,2048]{1,0:T(8,128)(2,1)S(1)} %copy-done.2, f32[2048]{0:T(1024)S(1)} %copy-done.4, f32[32]{0:T(128)S(1)} %add_rsqrt_fusion.2), kind=kOutput, calls=%fused_computation.54 | convolution fusion | flops 67780608 | bytes 2369664 | tf_op jit(solution)/shard_map/dot_general | solution.py:53
  15.3 8.2 %multiply_add_fusion = f32[32,4,128,128]{3,2,1,0:T(8,128)S(1)} fusion(f32[32,4,128,128]{3,2,1,0:T(8,128)} %param.21, f32[32,4,128]{2,1,0:T(4,128)S(1)} %mul.144, f32[32,4,128]{2,1,0:T(4,128)S(1)} %neg.60, f32[32,4,128]{2,1,0:T(4,128)S(1)} %exp.44), kind=kLoop, calls=%fused_computation | loop fusion | flops 6291456 | bytes 16973824 | tf_op jit(solution)/shard_map/add | solution.py:62
  23.5 0.0 copy-start.1
  23.6 7.3 %fusion.50 = f32[32,4,1,128]{3,2,1,0:T(1,128)S(1)} fusion(f32[32,4,128,1]{2,3,1,0:T(1,128)S(1)} %bitcast.54, f32[32,4,128,128]{3,2,1,0:T(8,128)S(1)} %multiply_add_fusion), kind=kOutput, calls=%fused_computation.59 | convolution fusion | flops 25165824 | bytes 8519680 | tf_op jit(solution)/shard_map/thk,thkv->thv/dot_general | solution.py:63
  30.8 0.1 multiply_reduce_fusion.1
  31.0 0.1 multiply_multiply_fusion
  31.1 3.8 %convolution_convert_fusion.2 = bf16[32,2048]{1,0:T(8,128)(2,1)} fusion(bf16[512,2048]{1,0:T(8,128)(2,1)} %param.29, f32[4,8,4,128]{3,2,1,0:T(4,128)S(1)} %bitcast.55, bf16[2048,512]{1,0:T(8,128)(2,1)} %param.26, bf16[32,2048]{1,0:T(8,128)(2,1)S(1)} %copy-done.2, f32[2048]{0:T(1024)S(1)} %copy-done.4, f32[32]{0:T(128)S(1)} %add_rsqrt_fusion.2), kind=kOutput, calls=%fused_computation.13 | convolution fusion | flops 134643712 | bytes 4530304 | tf_op jit(solution)/shard_map/dot_general | solution.py:66
  34.9 0.0 all-reduce.3.cloned.1.call-update
  35.0 0.1 copy.24
  35.0 0.1 reshape.93
  35.1 0.1 fusion.28
  35.2 0.1 reduce_window_sum.11
  35.3 0.2 select_reduce_fusion
  35.5 34.1 %all-reduce.3.cloned.1.call-done = bf16[32,2048]{1,0:T(8,128)(2,1)} async-done(((bf16[32,2048]{1,0:T(8,128)(2,1)}), bf16[32,2048]{1,0:T(8,128)(2,1)}) %all-reduce.3.cloned.1.call-update) | async-done | bytes 131088 | tf_op jit(solution)/shard_map/psum | solution.py:68
  69.6 1.1 multiply_reduce_fusion
  70.7 1.0 multiply_convert_fusion
  71.7 0.6 copy-done.3
  72.3 0.1 broadcast_in_dim.2
  72.5 0.1 reshape.94
  72.6 0.4 convolution_convert_fusion.1
  73.0 18.7 %all_to_all.15 = bf16[8,16,2048]{2,1,0:T(8,128)(2,1)S(1)} all-to-all(bf16[8,16,2048]{2,1,0:T(8,128)(2,1)S(1)} %bitcast.48), channel_id=1, replica_groups=mesh['ep'=8,'tp'=4] {'ep'}, dimensions={0} | all-to-all | bytes 1048576 | tf_op jit(solution)/shard_map/all_to_all | solution.py:96
  91.7 2.0 stack.2
  93.8 4.2 %all-to-all-start.2 = ((bf16[8,32,2048]{2,1,0:T(8,128)(2,1)}), bf16[8,32,2048]{2,1,0:T(8,128)(2,1)}, u32[]{:S(2)}, u32[]{:S(2)}) async-start(bf16[8,32,2048]{2,1,0:T(8,128)(2,1)} %stack.2), calls=%async_computation.2 | async-start | bytes 2097152 | tf_op jit(solution)/shard_map/all_to_all | solution.py:72
  98.0 0.2 all-reduce.5.cloned.1.call-start
  98.2 4.5 %fusion.4 = f32[128,1408]{1,0:T(8,128)} fusion(bf16[128,2048]{1,0:T(8,128)(2,1)S(1)} %bitcast.49, bf16[1,2048,1408]{2,1,0:T(8,128)(2,1)} %param.33), kind=kOutput, calls=%fused_computation.5 | convolution fusion | flops 738197504 | bytes 7012352 | tf_op jit(solution)/shard_map/dot_general | solution.py:99
  102.7 7.3 %fusion.12 = bf16[128,2048]{1,0:T(8,128)(2,1)} fusion(bf16[1,1408,2048]{2,1,0:T(8,128)(2,1)} %param.35, bf16[128,2048]{1,0:T(8,128)(2,1)S(1)} %bitcast.50, bf16[1,2048,1408]{2,1,0:T(8,128)(2,1)} %param.34, f32[128,1408]{1,0:T(8,128)} %fusion.4), kind=kOutput, calls=%fused_computation.11 | convolution fusion | flops 1477738496 | bytes 13303808 | tf_op jit(solution)/shard_map/dot_general | solution.py:102
  110.0 0.0 all-reduce.5.cloned.1.call-update
  110.0 0.0 reduce-scatter.2.cloned.1.call-start
  110.1 13.0 %all-to-all-done.2 = bf16[8,32,2048]{2,1,0:T(8,128)(2,1)} async-done(((bf16[8,32,2048]{2,1,0:T(8,128)(2,1)}), bf16[8,32,2048]{2,1,0:T(8,128)(2,1)}, u32[]{:S(2)}, u32[]{:S(2)}) %all-to-all-start.2) | async-done | bytes 1048608 | tf_op jit(solution)/shard_map/all_to_all | solution.py:72
  123.1 4.0 %fusion.51 = f32[256,704]{0,1:T(8,128)} fusion(bf16[256,2048]{1,0:T(8,128)(2,1)} %bitcast.10, bf16[2048,704]{0,1:T(8,128)(2,1)} %param.36), kind=kOutput, calls=%fused_computation.60 | convolution fusion | flops 738197504 | bytes 4653056 | tf_op jit(solution)/shard_map/dot_general | solution.py:78
  127.0 6.6 %convolution_convert_fusion = bf16[256,2048]{1,0:T(8,128)(2,1)} fusion(bf16[704,2048]{1,0:T(8,128)(2,1)S(1)} %copy-done, bf16[256,2048]{1,0:T(8,128)(2,1)} %bitcast.10, bf16[2048,704]{0,1:T(8,128)(2,1)} %param.37, f32[256,704]{0,1:T(8,128)} %fusion.51), kind=kOutput, calls=%fused_computation.7 | convolution fusion | flops 1478000640 | bytes 8585216 | tf_op jit(solution)/shard_map/dot_general | solution.py:83
  133.6 0.0 reduce-scatter.2.cloned.1.call-update
  133.6 10.4 %all-reduce.5.cloned.1.call-done = bf16[8,16,2048]{2,1,0:T(8,128)(2,1)} async-done(((bf16[8,16,2048]{2,1,0:T(8,128)(2,1)}), bf16[8,16,2048]{2,1,0:T(8,128)(2,1)}) %all-reduce.5.cloned.1.call-update) | async-done | bytes 524304 | tf_op jit(solution)/shard_map/psum | solution.py:104
  144.0 5.5 %all-to-all-start.1 = ((bf16[8,16,2048]{2,1,0:T(8,128)(2,1)}), bf16[8,16,2048]{2,1,0:T(8,128)(2,1)S(1)}, u32[]{:S(2)}, u32[]{:S(2)}) async-start(bf16[8,16,2048]{2,1,0:T(8,128)(2,1)} %all-reduce.5.cloned.1.call-done), calls=%async_computation.1 | async-start | bytes 1048576 | tf_op jit(solution)/shard_map/all_to_all | solution.py:106
  149.5 0.8 copy.25
  150.3 0.6 mul.164
  150.9 0.7 add_divide_fusion
  151.6 15.3 %all-to-all-done.1 = bf16[8,16,2048]{2,1,0:T(8,128)(2,1)S(1)} async-done(((bf16[8,16,2048]{2,1,0:T(8,128)(2,1)}), bf16[8,16,2048]{2,1,0:T(8,128)(2,1)S(1)}, u32[]{:S(2)}, u32[]{:S(2)}) %all-to-all-start.1) | async-done | bytes 524320 | tf_op jit(solution)/shard_map/all_to_all | solution.py:106
  166.9 1.8 convolution_multiply_fusion
  168.7 1.4 reshape.99
  170.0 1.4 reduce_sum.49
  171.4 41.4 %reduce-scatter.2.cloned.1.call-done = bf16[32,2048]{1,0:T(8,128)(2,1)} async-done(((bf16[256,2048]{1,0:T(8,128)(2,1)}), bf16[32,2048]{1,0:T(8,128)(2,1)}) %reduce-scatter.2.cloned.1.call-update) | async-done | bytes 131088 | tf_op jit(solution)/shard_map/reduce_scatter | solution.py:82
  212.8 1.8 add_convert_fusion
  (26 shorter events, 0.2 us)
Async XLA Ops:
  7.2 119.9 %copy-start = (bf16[704,2048]{1,0:T(8,128)(2,1)S(1)}, bf16[704,2048]{1,0:T(8,128)(2,1)}, u32[]{:S(2)}) copy-start(bf16[704,2048]{1,0:T(8,128)(2,1)} %param.38) | copy-start | bytes 8650756
  7.2 5.8 %copy-start.2 = (bf16[32,2048]{1,0:T(8,128)(2,1)S(1)}, bf16[32,2048]{1,0:T(8,128)(2,1)}, u32[]{:S(2)}) copy-start(bf16[32,2048]{1,0:T(8,128)(2,1)} %param.20) | copy-start | bytes 393220
  7.2 5.8 %copy-start.4 = (f32[2048]{0:T(1024)S(1)}, f32[2048]{0:T(1024)}, u32[]{:S(2)}) copy-start(f32[2048]{0:T(1024)} %param.22) | copy-start | bytes 24580
  7.2 5.7 %copy-start.7 = (f32[512]{0:T(512)S(1)}, f32[512]{0:T(512)}, u32[]{:S(2)}) copy-start(f32[512]{0:T(512)} %param.27) | copy-start | bytes 6148
  7.2 62.4 %all-reduce.3.cloned.1.call-start = ((), (), s32[]{:S(2)}) async-start(), calls=%async_computation.4 | async-start | bytes 262144 | tf_op jit(solution)/shard_map/psum | solution.py:68
  23.5 7.3 %copy-start.1 = (f32[32,4,128,128]{3,2,1,0:T(8,128)}, f32[32,4,128,128]{3,2,1,0:T(8,128)S(1)}, u32[]{:S(2)}) copy-start(f32[32,4,128,128]{3,2,1,0:T(8,128)S(1)} %multiply_add_fusion) | copy-start | bytes 25165828
  23.6 7.4 %copy-start.9 = (f32[128]{0:T(128)S(1)}, f32[128]{0:T(128)}, u32[]{:S(2)}) copy-start(f32[128]{0:T(128)} %param.28) | copy-start | bytes 1540
  30.8 4.1 %copy-start.8 = (s32[32,2]{0,1:T(2,128)S(1)}, s32[32,2]{0,1:T(2,128)}, u32[]{:S(2)}) copy-start(s32[32,2]{0,1:T(2,128)} %param.31) | copy-start | bytes 772
  30.8 39.9 %copy-start.5 = (f32[2048]{0:T(1024)S(1)}, f32[2048]{0:T(1024)}, u32[]{:S(2)}) copy-start(f32[2048]{0:T(1024)} %param.30) | copy-start | bytes 24580
  35.5 58.2 %copy-start.6 = (s32[64]{0:T(128)}, s32[64]{0:T(128)S(1)}, u32[]{:S(2)}) copy-start(s32[64]{0:T(128)S(1)} %multiply_add_fusion.1) | copy-start | bytes 772
  71.7 0.7 copy-start.3
  93.8 29.3 %all-to-all-start.2 = ((bf16[8,32,2048]{2,1,0:T(8,128)(2,1)}), bf16[8,32,2048]{2,1,0:T(8,128)(2,1)}, u32[]{:S(2)}, u32[]{:S(2)}) async-start(bf16[8,32,2048]{2,1,0:T(8,128)(2,1)} %stack.2), calls=%async_computation.2 | async-start | bytes 2097152 | tf_op jit(solution)/shard_map/all_to_all | solution.py:72
  98.0 46.0 %all-reduce.5.cloned.1.call-start = ((), (), s32[]{:S(2)}) async-start(), calls=%async_computation.5 | async-start | bytes 1048576 | tf_op jit(solution)/shard_map/psum | solution.py:104
  110.0 102.8 %reduce-scatter.2.cloned.1.call-start = ((), (), s32[]{:S(2)}) async-start(), calls=%async_computation.6 | async-start | bytes 1179648 | tf_op jit(solution)/shard_map/reduce_scatter | solution.py:82
  144.0 22.9 %all-to-all-start.1 = ((bf16[8,16,2048]{2,1,0:T(8,128)(2,1)}), bf16[8,16,2048]{2,1,0:T(8,128)(2,1)S(1)}, u32[]{:S(2)}, u32[]{:S(2)}) async-start(bf16[8,16,2048]{2,1,0:T(8,128)(2,1)} %all-reduce.5.cloned.1.call-done), calls=%async_computation.1 | async-start | bytes 1048576 | tf_op jit(solution)/shard_map/all_to_all | solution.py:106
Sparse Core Ops, SparseCore 0:
  35.1 34.4 all-reduce.2
  110.1 33.8 all-reduce.4
  147.4 65.3 reduce-scatter.1
